TPU v7x, 32 devices: a whole 2x2x4 slice. The times are simulated.
32 devices in a mesh: sp: 8 (over z, x), tp: 4 (over y, core).
Axes of the slice: x: 2, y: 2, z: 4, core: 2. Of those that a mesh axis runs over, the one named last changes fastest.
Arguments:
- layer_input: bfloat16 [4, 2048, 2048], P(None, ('sp', 'tp')), as said below
- key_weight: bfloat16 [2048, 384], replicated, may hold values from -0.125 to 0.125
- value_weight: bfloat16 [2048, 384], replicated, may hold values from -0.125 to 0.125
- queries: bfloat16 [24, 5, 64], P('sp'), may hold values from -6 to 6
- head_bias: float32 [6, 5], replicated, as said below
Outputs:
- stored: bfloat16 [24, 8, 256, 128], P('sp', None, 'tp')
- first_read: bfloat16 [24, 320], P('sp')
Inputs may be any that keep to these rules, and one draw needn't show every extreme that they name: `layer_input`: entries lie between -12.5 and 12.5. `head_bias`: entries lie between -1 minus the natural logarithm of 2048 and -3.
All inputs are finite; a program needn't handle non-finite values.
Results may differ from a plain program's by a relative error of at most 0.01.
Values may be sent and summed in bfloat16 or wider, within the bound.
A program may use at most 64 MiB of HBM per device.

v0:
```python
import math
import jax
import jax.numpy as jnp
from jax import lax
from jax.sharding import PartitionSpec as P

HD = 64
KVH = 6
GROUP = 5
EPS_NORM = 0.0001


def head_norm(summed):
    squares = jnp.mean(summed * summed, axis=-1, keepdims=True)
    return summed * lax.rsqrt(squares + EPS_NORM)


def shift_table(pair_ids, head_bias):
    heads_range = jnp.arange(KVH, dtype=jnp.int32)
    picker = (pair_ids[:, None] % KVH == heads_range[None, :]).astype(jnp.float32)
    return jnp.dot(picker, head_bias, precision=lax.Precision.HIGHEST)


def per_device(layer_input, key_weight, value_weight, queries, head_bias):
    seq_count, positions, model_width = layer_input.shape
    tokens_flat = layer_input.reshape(seq_count * positions, model_width)
    key_rows = (
        jnp.dot(tokens_flat, key_weight, preferred_element_type=jnp.float32)
        .astype(jnp.bfloat16)
        .reshape(seq_count, positions, KVH, HD)
    )
    value_rows = (
        jnp.dot(tokens_flat, value_weight, preferred_element_type=jnp.float32)
        .astype(jnp.bfloat16)
        .reshape(seq_count, positions, KVH, HD)
    )
    kv_rows = (
        jnp.concatenate([key_rows, value_rows], axis=-1)
        .transpose(0, 2, 1, 3)
        .reshape(seq_count * KVH, 1, positions, 2 * HD)
    )
    stored = lax.all_to_all(kv_rows, "sp", split_axis=0, concat_axis=1, tiled=True)
    score_scale = 1.0 / math.sqrt(HD)
    local_pairs = queries.shape[0]
    pair_ids = lax.axis_index("sp") * local_pairs + jnp.arange(local_pairs, dtype=jnp.int32)
    head_shift = shift_table(pair_ids, head_bias)
    scores = (
        jnp.einsum("pgc,pbtc->pgbt", queries, stored[..., :HD], preferred_element_type=jnp.float32)
        * score_scale
        + head_shift[:, :, None, None]
    )
    keep_log = jax.nn.log_sigmoid(-scores)
    totals = jnp.sum(keep_log, axis=3)
    gathered = lax.all_gather(totals[None], "tp", axis=0, tiled=True)
    later_mask = (jnp.arange(gathered.shape[0], dtype=jnp.int32) > lax.axis_index("tp")).astype(
        jnp.float32
    )
    later_inside = jnp.sum(gathered * later_mask[:, None, None, None], axis=0)
    block_sums = jnp.sum(gathered, axis=0)
    later_blocks = lax.cumsum(block_sums, axis=2, reverse=True) - block_sums
    suffix_log = (
        lax.cumsum(keep_log, axis=3, reverse=True)
        - keep_log
        + (later_inside + later_blocks)[..., None]
    )
    weights = jnp.exp(jax.nn.log_sigmoid(scores) + suffix_log).astype(jnp.bfloat16)
    partial_value = jnp.einsum(
        "pgbt,pbtc->pgc", weights, stored[..., HD:], preferred_element_type=jnp.float32
    )
    summed = lax.psum(partial_value, "tp")
    first_read = head_norm(summed).reshape(local_pairs, GROUP * HD).astype(jnp.bfloat16)
    return (stored, first_read)


def solution(mesh):
    in_specs = (P(None, ("sp", "tp"), None), P(), P(), P("sp", None, None), P())
    out_specs = (P("sp", None, "tp", None), P("sp", None))
    return jax.shard_map(
        per_device, mesh=mesh, in_specs=in_specs, out_specs=out_specs, check_vma=False
    )
```

profile of v0, /device:TPU:0, one launch (start us, length us, event | category | flops | bytes accessed | tf_op | source)
XLA Modules:
  0.0 53.3 jit_solution(13283465844717739790)
XLA Ops:
  0.6 0.0 copy-start
  0.6 1.4 %copy-done = bf16[2048,384]{1,0:T(8,128)(2,1)S(1)} copy-done((bf16[2048,384]{1,0:T(8,128)(2,1)S(1)}, bf16[2048,384]{1,0:T(8,128)(2,1)}, u32[]{:S(2)}) %copy-start) | copy-done | bytes 1572888
  2.0 0.0 copy-start.2
  2.0 2.0 %convolution_convert_fusion.1 = bf16[256,384]{1,0:T(8,128)(2,1)S(1)} fusion(bf16[256,2048]{1,0:T(8,128)(2,1)} %bitcast.33, bf16[2048,384]{1,0:T(8,128)(2,1)S(1)} %copy-done), kind=kOutput, calls=%fused_computation.1 | convolution fusion | flops 402751488 | bytes 2818048 | tf_op jit(solution)/shard_map/dot_general | solution.py:28
  4.1 0.1 copy.26
  4.2 0.2 reshape.69
  4.4 0.0 copy-done.2
  4.4 2.1 %convolution_convert_fusion = bf16[256,384]{1,0:T(8,128)(2,1)S(1)} fusion(bf16[256,2048]{1,0:T(8,128)(2,1)S(1)} %bitcast.34, bf16[2048,384]{1,0:T(8,128)(2,1)} %param.7), kind=kOutput, calls=%fused_computation | convolution fusion | flops 402751488 | bytes 2818048 | tf_op jit(solution)/shard_map/dot_general | solution.py:33
  6.6 0.1 copy.27
  6.7 0.2 reshape.70
  6.9 0.0 copy-start.4
  6.9 0.6 %maximum_bitcast_fusion = bf16[4,6,64,128]{2,0,3,1:T(4,128)(2,1)S(1)} fusion(bf16[4,64,6,64]{1,0,3,2:T(4,128)(2,1)S(1)} %reshape.70, bf16[4,64,6,64]{1,0,3,2:T(4,128)(2,1)S(1)} %reshape.69), kind=kLoop, calls=%fused_computation.6 | loop fusion | flops 196608 | bytes 786432 | tf_op jit(solution)/shard_map/transpose | solution.py:39
  7.6 0.0 copy-start.3
  7.6 1.2 %copy.28 = bf16[4,6,64,128]{3,2,1,0:T(8,128)(2,1)} copy(bf16[4,6,64,128]{2,0,3,1:T(4,128)(2,1)S(1)} %maximum_bitcast_fusion) | data formatting | bytes 786432 | tf_op jit(solution)/shard_map/transpose | solution.py:39
  8.7 7.3 %all-to-all-start = ((bf16[24,1,64,128]{3,2,1,0:T(8,128)(2,1)}), bf16[24,1,64,128]{3,2,1,0:T(8,128)(2,1)S(1)}, u32[]{:S(2)}, u32[]{:S(2)}) async-start(bf16[24,1,64,128]{3,2,1,0:T(8,128)(2,1)} %bitcast.3), calls=%async_computation | async-start | bytes 786432 | tf_op jit(solution)/shard_map/all_to_all | solution.py:42
  16.0 0.0 copy-done.4
  16.1 0.2 fusion.15
  16.2 11.5 %all-to-all-done = bf16[24,1,64,128]{3,2,1,0:T(8,128)(2,1)S(1)} async-done(((bf16[24,1,64,128]{3,2,1,0:T(8,128)(2,1)}), bf16[24,1,64,128]{3,2,1,0:T(8,128)(2,1)S(1)}, u32[]{:S(2)}, u32[]{:S(2)}) %all-to-all-start) | async-done | bytes 393248 | tf_op jit(solution)/shard_map/all_to_all | solution.py:42
  27.7 0.0 copy-start.1
  27.7 0.0 copy-done.3
  27.8 0.5 fusion.9
  28.3 0.1 copy.34
  28.4 5.2 %all-gather = f32[12,5,8]{2,1,0:T(8,128)S(1)} all-gather(f32[3,5,8]{2,1,0:T(8,128)S(1)} %copy.34), channel_id=2, replica_groups=mesh['sp'=8,'tp'=4] {'tp'}, dimensions={0}, use_global_device_ids=true | all-gather | bytes 2400 | tf_op jit(solution)/shard_map/all_gather | solution.py:54
  33.6 0.1 fusion.19
  33.7 0.5 reduce_window_sum.21
  34.2 0.1 copy.35
  34.3 6.4 %reduce_window_sum.20 = f32[3,5,8,64]{3,2,1,0:T(8,128)S(1)} reduce-window(f32[3,5,8,64]{3,2,1,0:T(8,128)S(1)} %copy.32, f32[]{:T(128)} %constant.36.clone.1), window={size=1x1x1x64 pad=0_0x0_0x0_0x0_63}, to_apply=%region_0.1 | reduce-window | flops 483840 | bytes 61444 | tf_op jit(solution)/shard_map/per_device/reduce_window_sum | solution.py:62
  40.7 0.4 convolution_bitcast_fusion
  41.1 11.4 %psum.7 = f32[3,5,64]{2,1,0:T(8,128)S(1)} all-reduce(f32[3,5,64]{2,1,0:T(8,128)S(1)} %convolution_bitcast_fusion), channel_id=1, replica_groups=mesh['sp'=8,'tp'=4] {'tp'}, use_global_device_ids=true, to_apply=%region_5.6 | all-reduce | flops 960 | bytes 7680 | tf_op jit(solution)/shard_map/psum | solution.py:70
  52.5 0.1 multiply_reduce_fusion.1
  52.6 0.1 multiply_convert_fusion
  52.7 0.7 %convert_element_type.28 = bf16[3,320]{1,0:T(4,128)(2,1)} reshape(bf16[3,5,64]{2,1,0:T(8,128)(2,1)S(1)} %multiply_convert_fusion) | data formatting | bytes 3840 | tf_op jit(solution)/shard_map/convert_element_type | solution.py:71
  53.3 0.0 copy-done.1
  (7 shorter events, 0.1 us)
Async XLA Ops:
  0.6 1.4 %copy-start = (bf16[2048,384]{1,0:T(8,128)(2,1)S(1)}, bf16[2048,384]{1,0:T(8,128)(2,1)}, u32[]{:S(2)}) copy-start(bf16[2048,384]{1,0:T(8,128)(2,1)} %param.6) | copy-start | bytes 4718596
  2.0 2.4 %copy-start.2 = (bf16[4,64,2048]{2,1,0:T(8,128)(2,1)S(1)}, bf16[4,64,2048]{2,1,0:T(8,128)(2,1)}, u32[]{:S(2)}) copy-start(bf16[4,64,2048]{2,1,0:T(8,128)(2,1)} %param.5) | copy-start | bytes 3145732
  6.9 9.1 %copy-start.4 = (f32[6,5]{1,0:T(8,128)S(1)}, f32[6,5]{1,0:T(8,128)}, u32[]{:S(2)}) copy-start(f32[6,5]{1,0:T(8,128)} %param.9) | copy-start | bytes 364
  7.6 20.2 %copy-start.3 = (bf16[3,5,64]{2,0,1:T(4,128)(2,1)S(1)}, bf16[3,5,64]{2,0,1:T(4,128)(2,1)}, u32[]{:S(2)}) copy-start(bf16[3,5,64]{2,0,1:T(4,128)(2,1)} %param.8) | copy-start | bytes 5764
  8.7 19.0 %all-to-all-start = ((bf16[24,1,64,128]{3,2,1,0:T(8,128)(2,1)}), bf16[24,1,64,128]{3,2,1,0:T(8,128)(2,1)S(1)}, u32[]{:S(2)}, u32[]{:S(2)}) async-start(bf16[24,1,64,128]{3,2,1,0:T(8,128)(2,1)} %bitcast.3), calls=%async_computation | async-start | bytes 786432 | tf_op jit(solution)/shard_map/all_to_all | solution.py:42
  27.7 25.6 %copy-start.1 = (bf16[8,3,1,64,128]{4,3,0,1,2:T(8,128)(2,1)}, bf16[8,3,1,64,128]{4,3,0,1,2:T(8,128)(2,1)S(1)}, u32[]{:S(2)}) copy-start(bf16[8,3,1,64,128]{4,3,0,1,2:T(8,128)(2,1)S(1)} %copy.51) | copy-start | bytes 1179652
where the time goes:
time: 53.7 us; the launch traced here: 53.3 us
  blocking collectives  16.6 us (31%)
  waiting for transfers between devices  11.5 us (21%)
  other arithmetic  7.8 us (15%)
  starting transfers between devices  7.28 us (14%)
  matrix products  5.23 us (10%)
  local copies, waits for them, and re-layouts  4.2 us (8%)
  between operations  0.75 us (1%)
    all_to_all x1, waiting for transfers between devices, per_device(): lax.all_to_all(kv_rows, 'sp', split_axis=0, concat_axis=1, tiled=True)  11.5 us
    psum x1, blocking collectives, per_device(): summed = lax.psum(partial_value, 'tp')  11.4 us
    all_to_all x1, starting transfers between devices, per_device(): lax.all_to_all(kv_rows, 'sp', split_axis=0, concat_axis=1, tiled=True)  7.28 us
    another operation x1, other arithmetic, per_device(): lax.cumsum(keep_log, axis=3, reverse=True) - keep_log  6.41 us
    all_gather x1, blocking collectives, per_device(): gathered = lax.all_gather(totals[None], 'tp', axis=0, tiled=True)  5.21 us
    dot_general x1, matrix products, per_device(): jnp.dot(tokens_flat, value_weight, preferred_element_type=jnp.float32)  2.12 us
    dot_general x1, matrix products, per_device(): jnp.dot(tokens_flat, key_weight, preferred_element_type=jnp.float32)  2.02 us
    unnamed x10, local copies, waits for them, and re-layouts  1.43 us
  transfers between devices with their start and end apart: 1, of which 1 were waited for; matrix products, arithmetic and copies ran while one was open for 0% of the time, Pallas kernels for 0%

commit v1 on v0

--- a/solution.py
+++ b/solution.py
@@ -67,7 +67,9 @@
     partial_value = jnp.einsum(
         "pgbt,pbtc->pgc", weights, stored[..., HD:], preferred_element_type=jnp.float32
     )
-    summed = lax.psum(partial_value, "tp")
+    summed = partial_value
+    for hop in (1, 2):
+        summed = summed + lax.ppermute(summed, "tp", [(dev, dev ^ hop) for dev in range(4)])
     first_read = head_norm(summed).reshape(local_pairs, GROUP * HD).astype(jnp.bfloat16)
     return (stored, first_read)
 

time: 53.7 us -> 47.1 us (0.88)
  blocking collectives: 16.6 us -> 5.21 us
  waiting for transfers between devices: 11.5 us -> 14.5 us
  starting transfers between devices: 7.28 us -> 9.18 us
    psum x1 -> x0, blocking collectives: 11.4 us -> none  [per_device(): summed = lax.psum(partial_value, 'tp')]
    ppermute x0 -> x2, waiting for transfers between devices: none -> 3.01 us  [per_device(): lax.ppermute(summed, 'tp', [(dev, dev ^ hop) for dev in range(4)])]
    ppermute x0 -> x2, starting transfers between devices: none -> 1.89 us  [per_device(): lax.ppermute(summed, 'tp', [(dev, dev ^ hop) for dev in range(4)])]
  transfers between devices with their start and end apart: 1 -> 3, of which waited for: 1 -> 3; matrix products, arithmetic and copies ran while one was open for 0% -> 0% of each run, Pallas kernels for 0% -> 0%
where the time goes in v1:
time: 47.1 us; the launch traced here: 46.8 us
  waiting for transfers between devices  14.5 us (31%)
  starting transfers between devices  9.18 us (19%)
  other arithmetic  7.8 us (17%)
  matrix products  5.23 us (11%)
  blocking collectives  5.21 us (11%)
  local copies, waits for them, and re-layouts  4.2 us (9%)
  between operations  0.76 us (2%)
    all_to_all x1, waiting for transfers between devices, per_device(): lax.all_to_all(kv_rows, 'sp', split_axis=0, concat_axis=1, tiled=True)  11.5 us
    all_to_all x1, starting transfers between devices, per_device(): lax.all_to_all(kv_rows, 'sp', split_axis=0, concat_axis=1, tiled=True)  7.28 us
    another operation x1, other arithmetic, per_device(): lax.cumsum(keep_log, axis=3, reverse=True) - keep_log  6.41 us
    all_gather x1, blocking collectives, per_device(): gathered = lax.all_gather(totals[None], 'tp', axis=0, tiled=True)  5.21 us
    ppermute x2, waiting for transfers between devices, per_device(): lax.ppermute(summed, 'tp', [(dev, dev ^ hop) for dev in range(4)])  3.01 us
    dot_general x1, matrix products, per_device(): jnp.dot(tokens_flat, value_weight, preferred_element_type=jnp.float32)  2.12 us
    dot_general x1, matrix products, per_device(): jnp.dot(tokens_flat, key_weight, preferred_element_type=jnp.float32)  2.02 us
    ppermute x2, starting transfers between devices, per_device(): lax.ppermute(summed, 'tp', [(dev, dev ^ hop) for dev in range(4)])  1.89 us
  transfers between devices with their start and end apart: 3, of which 3 were waited for; matrix products, arithmetic and copies ran while one was open for 0% of the time, Pallas kernels for 0%

profile of v1, /device:TPU:0, one launch (start us, length us, event | category | flops | bytes accessed | tf_op | source)
XLA Modules:
  0.0 46.8 jit_solution(7169330504147404881)
XLA Ops:
  0.6 0.0 copy-start
  0.6 1.4 %copy-done = bf16[2048,384]{1,0:T(8,128)(2,1)S(1)} copy-done((bf16[2048,384]{1,0:T(8,128)(2,1)S(1)}, bf16[2048,384]{1,0:T(8,128)(2,1)}, u32[]{:S(2)}) %copy-start) | copy-done | bytes 1572888
  2.0 0.0 copy-start.2
  2.0 2.0 %convolution_convert_fusion.1 = bf16[256,384]{1,0:T(8,128)(2,1)S(1)} fusion(bf16[256,2048]{1,0:T(8,128)(2,1)} %bitcast.33, bf16[2048,384]{1,0:T(8,128)(2,1)S(1)} %copy-done), kind=kOutput, calls=%fused_computation.1 | convolution fusion | flops 402751488 | bytes 2818048 | tf_op jit(solution)/shard_map/dot_general | solution.py:28
  4.1 0.1 copy.26
  4.2 0.2 reshape.69
  4.4 0.0 copy-done.2
  4.4 2.1 %convolution_convert_fusion = bf16[256,384]{1,0:T(8,128)(2,1)S(1)} fusion(bf16[256,2048]{1,0:T(8,128)(2,1)S(1)} %bitcast.34, bf16[2048,384]{1,0:T(8,128)(2,1)} %param.7), kind=kOutput, calls=%fused_computation | convolution fusion | flops 402751488 | bytes 2818048 | tf_op jit(solution)/shard_map/dot_general | solution.py:33
  6.6 0.1 copy.27
  6.7 0.2 reshape.70
  6.9 0.0 copy-start.4
  6.9 0.6 %maximum_bitcast_fusion = bf16[4,6,64,128]{2,0,3,1:T(4,128)(2,1)S(1)} fusion(bf16[4,64,6,64]{1,0,3,2:T(4,128)(2,1)S(1)} %reshape.70, bf16[4,64,6,64]{1,0,3,2:T(4,128)(2,1)S(1)} %reshape.69), kind=kLoop, calls=%fused_computation.6 | loop fusion | flops 196608 | bytes 786432 | tf_op jit(solution)/shard_map/transpose | solution.py:39
  7.6 0.0 copy-start.3
  7.6 1.2 %copy.28 = bf16[4,6,64,128]{3,2,1,0:T(8,128)(2,1)} copy(bf16[4,6,64,128]{2,0,3,1:T(4,128)(2,1)S(1)} %maximum_bitcast_fusion) | data formatting | bytes 786432 | tf_op jit(solution)/shard_map/transpose | solution.py:39
  8.7 7.3 %all-to-all-start = ((bf16[24,1,64,128]{3,2,1,0:T(8,128)(2,1)}), bf16[24,1,64,128]{3,2,1,0:T(8,128)(2,1)S(1)}, u32[]{:S(2)}, u32[]{:S(2)}) async-start(bf16[24,1,64,128]{3,2,1,0:T(8,128)(2,1)} %bitcast.3), calls=%async_computation | async-start | bytes 786432 | tf_op jit(solution)/shard_map/all_to_all | solution.py:42
  16.0 0.0 copy-done.4
  16.1 0.2 fusion.15
  16.2 11.5 %all-to-all-done = bf16[24,1,64,128]{3,2,1,0:T(8,128)(2,1)S(1)} async-done(((bf16[24,1,64,128]{3,2,1,0:T(8,128)(2,1)}), bf16[24,1,64,128]{3,2,1,0:T(8,128)(2,1)S(1)}, u32[]{:S(2)}, u32[]{:S(2)}) %all-to-all-start) | async-done | bytes 393248 | tf_op jit(solution)/shard_map/all_to_all | solution.py:42
  27.7 0.0 copy-start.1
  27.7 0.0 copy-done.3
  27.8 0.5 %fusion.9 = (f32[3,5,8]{1,2,0:T(8,128)S(1)}, f32[3,5,8,64]{3,1,2,0:T(8,128)S(1)}, f32[3,5,8,64]{3,1,2,0:T(8,128)S(1)}) fusion(f32[3,5]{1,0:T(4,128)S(1)} %fusion.15, bf16[3,5,64,1]{2,0,1,3:T(4,128)(2,1)S(1)} %bitcast.35, bf16[3,8,64,128]{3,2,1,0:T(8,128)(2,1)S(1)} %bitcast.29), kind=kOutput, calls=%fused_computation.18 | convolution fusion | flops 1059720 | bytes 457116 | tf_op jit(solution)/shard_map/pgc,pbtc->pgbt/dot_general | solution.py:48
  28.3 0.1 copy.34
  28.4 5.2 %all-gather = f32[12,5,8]{2,1,0:T(8,128)S(1)} all-gather(f32[3,5,8]{2,1,0:T(8,128)S(1)} %copy.34), channel_id=2, replica_groups=mesh['sp'=8,'tp'=4] {'tp'}, dimensions={0}, use_global_device_ids=true | all-gather | bytes 2400 | tf_op jit(solution)/shard_map/all_gather | solution.py:54
  33.6 0.1 fusion.19
  33.7 0.5 %reduce_window_sum.21 = f32[3,5,8]{2,1,0:T(8,128)S(1)} reduce-window(f32[3,5,8]{2,1,0:T(8,128)S(1)} %get-tuple-element.2, f32[]{:T(128)} %constant.36.clone.1), window={size=1x1x8 pad=0_0x0_0x0_7}, to_apply=%region_4.5 | reduce-window | flops 840 | bytes 964 | tf_op jit(solution)/shard_map/per_device/reduce_window_sum | solution.py:60
  34.2 0.1 copy.35
  34.3 6.4 %reduce_window_sum.20 = f32[3,5,8,64]{3,2,1,0:T(8,128)S(1)} reduce-window(f32[3,5,8,64]{3,2,1,0:T(8,128)S(1)} %copy.32, f32[]{:T(128)} %constant.36.clone.1), window={size=1x1x1x64 pad=0_0x0_0x0_0x0_63}, to_apply=%region_0.1 | reduce-window | flops 483840 | bytes 61444 | tf_op jit(solution)/shard_map/per_device/reduce_window_sum | solution.py:62
  40.7 0.4 convolution_bitcast_fusion
  41.1 0.4 collective-permute-start
  41.5 0.8 %collective-permute-done = f32[3,5,64]{2,1,0:T(8,128)S(1)} collective-permute-done((f32[3,5,64]{2,1,0:T(8,128)S(1)}, f32[3,5,64]{2,1,0:T(8,128)S(1)}, u32[]{:S(2)}, u32[]{:S(2)}) %collective-permute-start) | collective-permute-done | bytes 3872 | tf_op jit(solution)/shard_map/ppermute | solution.py:72
  42.3 1.5 %collective-permute-start.1 = (f32[3,5,64]{2,1,0:T(8,128)S(1)}, f32[3,5,64]{2,1,0:T(8,128)S(1)}, u32[]{:S(2)}, u32[]{:S(2)}) collective-permute-start(f32[3,5,64]{2,1,0:T(8,128)S(1)} %add.84), channel_id=1, source_target_pairs={{0,2},{1,3},{2,0},{3,1},{4,6},{5,7},{6,4},{7,5},{8,10},{9,11},{10,... | collective-permute-start | bytes 11528 | tf_op jit(solution)/shard_map/ppermute | solution.py:72
  43.8 2.2 %collective-permute-done.1 = f32[3,5,64]{2,1,0:T(8,128)S(1)} collective-permute-done((f32[3,5,64]{2,1,0:T(8,128)S(1)}, f32[3,5,64]{2,1,0:T(8,128)S(1)}, u32[]{:S(2)}, u32[]{:S(2)}) %collective-permute-start.1) | collective-permute-done | bytes 3872 | tf_op jit(solution)/shard_map/ppermute | solution.py:72
  46.0 0.1 multiply_reduce_fusion.1
  46.1 0.1 multiply_convert_fusion
  46.2 0.7 %convert_element_type.28 = bf16[3,320]{1,0:T(4,128)(2,1)} reshape(bf16[3,5,64]{2,1,0:T(8,128)(2,1)S(1)} %multiply_convert_fusion) | data formatting | bytes 3840 | tf_op jit(solution)/shard_map/convert_element_type | solution.py:73
  46.8 0.0 copy-done.1
  (8 shorter events, 0.1 us)
Async XLA Ops:
  0.6 1.4 %copy-start = (bf16[2048,384]{1,0:T(8,128)(2,1)S(1)}, bf16[2048,384]{1,0:T(8,128)(2,1)}, u32[]{:S(2)}) copy-start(bf16[2048,384]{1,0:T(8,128)(2,1)} %param.6) | copy-start | bytes 4718596
  2.0 2.4 %copy-start.2 = (bf16[4,64,2048]{2,1,0:T(8,128)(2,1)S(1)}, bf16[4,64,2048]{2,1,0:T(8,128)(2,1)}, u32[]{:S(2)}) copy-start(bf16[4,64,2048]{2,1,0:T(8,128)(2,1)} %param.5) | copy-start | bytes 3145732
  6.9 9.1 %copy-start.4 = (f32[6,5]{1,0:T(8,128)S(1)}, f32[6,5]{1,0:T(8,128)}, u32[]{:S(2)}) copy-start(f32[6,5]{1,0:T(8,128)} %param.9) | copy-start | bytes 364
  7.6 20.2 %copy-start.3 = (bf16[3,5,64]{2,0,1:T(4,128)(2,1)S(1)}, bf16[3,5,64]{2,0,1:T(4,128)(2,1)}, u32[]{:S(2)}) copy-start(bf16[3,5,64]{2,0,1:T(4,128)(2,1)} %param.8) | copy-start | bytes 5764
  8.7 19.0 %all-to-all-start = ((bf16[24,1,64,128]{3,2,1,0:T(8,128)(2,1)}), bf16[24,1,64,128]{3,2,1,0:T(8,128)(2,1)S(1)}, u32[]{:S(2)}, u32[]{:S(2)}) async-start(bf16[24,1,64,128]{3,2,1,0:T(8,128)(2,1)} %bitcast.3), calls=%async_computation | async-start | bytes 786432 | tf_op jit(solution)/shard_map/all_to_all | solution.py:42
  27.7 19.1 %copy-start.1 = (bf16[8,3,1,64,128]{4,3,0,1,2:T(8,128)(2,1)}, bf16[8,3,1,64,128]{4,3,0,1,2:T(8,128)(2,1)S(1)}, u32[]{:S(2)}) copy-start(bf16[8,3,1,64,128]{4,3,0,1,2:T(8,128)(2,1)S(1)} %copy.51) | copy-start | bytes 1179652
  41.1 1.2 %collective-permute-start = (f32[3,5,64]{2,1,0:T(8,128)S(1)}, f32[3,5,64]{2,1,0:T(8,128)S(1)}, u32[]{:S(2)}, u32[]{:S(2)}) collective-permute-start(f32[3,5,64]{2,1,0:T(8,128)S(1)} %convolution_bitcast_fusion), channel_id=1, source_target_pairs={{0,1},{1,0},{2,3},{3,2},{4,5},{5,4},{6,7},{7,6},{8,9},{9,8},{10,11... | collective-permute-start | bytes 11528 | tf_op jit(solution)/shard_map/ppermute | solution.py:72
  42.3 3.7 %collective-permute-start.1 = (f32[3,5,64]{2,1,0:T(8,128)S(1)}, f32[3,5,64]{2,1,0:T(8,128)S(1)}, u32[]{:S(2)}, u32[]{:S(2)}) collective-permute-start(f32[3,5,64]{2,1,0:T(8,128)S(1)} %add.84), channel_id=1, source_target_pairs={{0,2},{1,3},{2,0},{3,1},{4,6},{5,7},{6,4},{7,5},{8,10},{9,11},{10,... | collective-permute-start | bytes 11528 | tf_op jit(solution)/shard_map/ppermute | solution.py:72
